TPU v7x, 32 devices: a whole 2x2x4 slice. The times are simulated.
32 devices in a mesh: sp: 8 (over z, x), tp: 4 (over y, core).
Axes of the slice: x: 2, y: 2, z: 4, core: 2. Of those that a mesh axis runs over, the one named last changes fastest.
Arguments:
- residual: bfloat16 [4096, 2048], P(('sp', 'tp')), may hold values from -6 to 6
- conv_value: bfloat16 [4096, 1024], P('sp', 'tp'), may hold values from -6 to 6
- conv_gate: bfloat16 [4096, 1024], P('sp', 'tp'), may hold values from -9 to 9
- segments: int32 [4096], P('sp'), may hold values from 0 to 3, never falling along the last dimension, each value on 1 to 2048 neighbouring positions
- conv_weight: float32 [31, 1024], P(None, 'tp'), may hold values from -1 to 1
- norm_gain: float32 [1024], P('tp'), may hold values from 0.1 to 1.9
- norm_shift: float32 [1024], P('tp'), may hold values from -3 to 3
- out_weight: bfloat16 [1024, 2048], replicated, may hold values from -0.1875 to 0.1875
- ffn_gain: float32 [2048], replicated, may hold values from 0.1 to 1.9
- routes: int32 [4096, 2], P('sp'), may hold values from 0 to 7, all different within a row; in each aligned block of 128 rows (0 to 127, 128 to 255, ...) at most 64 rows name the same one
- route_weights: float32 [4096, 2], P('sp'), may hold values from 0.2 to 1
- w_gate: bfloat16 [8, 2048, 1024], P('sp', None, 'tp'), may hold values from -0.125 to 0.125
- w_up: bfloat16 [8, 2048, 1024], P('sp', None, 'tp'), may hold values from -0.125 to 0.125
- w_down: bfloat16 [8, 1024, 2048], P('sp', 'tp'), may hold values from -0.1875 to 0.1875
Outputs:
- layer_out: bfloat16 [4096, 2048], P(('sp', 'tp'))
Inputs may be any that keep to these rules, and one draw needn't show every extreme that they name: `routes`: within the rows of one device (aligned blocks of 512 / 4 rows), no expert is named more than 64 times; the two experts of a row differ. `segments`: document numbers never fall along the sequence.
All inputs are finite; a program needn't handle non-finite values.
Results may differ from a plain program's by a relative error of at most 0.007.
Values may be sent and summed in bfloat16 or wider, within the bound.
A program may use at most 128 MiB of HBM per device.

v0:
```python
import jax
import jax.numpy as jnp
from jax import lax
from jax.sharding import PartitionSpec as P

DC = 1024
CONV_GROUPS = 8


def passed_along(value, axis, steps):
    count = lax.axis_size(axis)
    initial, last = (max(0, -steps), min(count, count - steps))
    return lax.ppermute(value, axis, [(source, source + steps) for source in range(initial, last)])


def slot_numbers(block_routes, capacity, experts_n):
    route_pairs = block_routes.reshape(block_routes.shape[:-2] + (-1,))
    onehot = (route_pairs[..., None] == jnp.arange(experts_n, dtype=jnp.int32)).astype(jnp.int32)
    slot_rank = jnp.sum((jnp.cumsum(onehot, axis=-2) - onehot) * onehot, axis=-1)
    return (route_pairs * capacity + slot_rank).reshape(block_routes.shape)


def dispatch_matrix(slot_ids, slot_total):
    numbers = jnp.arange(slot_total, dtype=jnp.int32)[:, None, None]
    matches = jnp.any(numbers == slot_ids[..., None, :, :], axis=-1)
    return matches.astype(jnp.bfloat16)


def shards(
    residual,
    conv_value,
    conv_gate,
    segments,
    conv_weight,
    norm_gain,
    norm_shift,
    out_weight,
    ffn_gain,
    routes,
    route_weights,
    w_gate,
    w_up,
    w_down,
):
    tok_dev, local_channels = conv_value.shape
    reach = conv_weight.shape[0] - 1
    whole_gate, whole_up = (
        lax.all_gather(w_gate[0], "tp", axis=1, tiled=True),
        lax.all_gather(w_up[0], "tp", axis=1, tiled=True),
    )
    whole_down = lax.all_gather(w_down[0], "tp", axis=0, tiled=True)
    gated = (conv_value.astype(jnp.float32) * jax.nn.sigmoid(conv_gate.astype(jnp.float32))).astype(
        jnp.bfloat16
    )
    rim_prev, seg_prev = passed_along(
        (gated[tok_dev - reach :], segments[tok_dev - reach :]), "sp", 1
    )
    extended = jnp.concatenate([rim_prev, gated], 0).astype(jnp.float32)
    seg_ext = jnp.concatenate([seg_prev, segments], 0)
    convolved = jnp.zeros((tok_dev, local_channels), jnp.float32)
    for offset in range(reach + 1):
        same_doc = (seg_ext[offset : offset + tok_dev] == segments)[:, None]
        convolved = convolved + jnp.where(
            same_doc, extended[offset : offset + tok_dev] * conv_weight[offset], 0.0
        )
    group_size = DC // CONV_GROUPS
    grouped = convolved.reshape(tok_dev, local_channels // group_size, group_size)
    group_mean = jnp.mean(grouped, axis=-1, keepdims=True)
    group_var = jnp.mean(jnp.square(grouped - group_mean), axis=-1, keepdims=True)
    scaled = ((grouped - group_mean) * lax.rsqrt(group_var + 1e-05)).reshape(
        tok_dev, local_channels
    ) * norm_gain + norm_shift
    conv_out = jax.nn.silu(scaled).astype(jnp.bfloat16)
    columns = lax.axis_size("tp")
    column = lax.axis_index("tp")
    rows_own = tok_dev // columns
    weight_rows = lax.dynamic_slice_in_dim(out_weight, column * local_channels, local_channels, 0)
    mixed = lax.psum_scatter(
        jnp.dot(conv_out, weight_rows, preferred_element_type=jnp.float32),
        "tp",
        scatter_dimension=0,
        tiled=True,
    )
    stream = residual.astype(jnp.float32) + lax.optimization_barrier(
        mixed.astype(jnp.bfloat16)
    ).astype(jnp.float32)
    normed = (
        stream * lax.rsqrt(jnp.mean(stream * stream, axis=-1, keepdims=True) + 1e-06) * ffn_gain
    ).astype(jnp.bfloat16)
    experts_n = lax.axis_size("sp")
    top_count = routes.shape[1]
    model_width = normed.shape[1]
    capacity = max(2, 2 * tok_dev * top_count // (columns * experts_n))
    slot_total = experts_n * capacity
    own_routes = lax.dynamic_slice_in_dim(routes, column * rows_own, rows_own, 0)
    own_weights = lax.dynamic_slice_in_dim(route_weights, column * rows_own, rows_own, 0)
    own_slots = slot_numbers(own_routes, capacity, experts_n)
    routing_table = dispatch_matrix(own_slots, slot_total)
    outgoing = jnp.dot(routing_table, normed, preferred_element_type=jnp.float32).astype(
        jnp.bfloat16
    )
    outgoing = outgoing.reshape(experts_n, capacity, model_width)
    arrived = lax.all_to_all(outgoing, "sp", split_axis=0, concat_axis=1, tiled=True).reshape(
        slot_total, model_width
    )
    gate_act = jnp.dot(arrived, whole_gate, preferred_element_type=jnp.float32)
    up_act = jnp.dot(arrived, whole_up, preferred_element_type=jnp.float32)
    hidden = (jax.nn.silu(gate_act) * up_act).astype(jnp.bfloat16)
    summed = jnp.dot(hidden, whole_down, preferred_element_type=jnp.float32)
    expert_out = summed.astype(jnp.bfloat16).reshape(experts_n, capacity, model_width)
    returned = lax.all_to_all(expert_out, "sp", split_axis=0, concat_axis=0, tiled=True).reshape(
        slot_total, model_width
    )
    combined = stream
    for member in range(top_count):
        chosen = jnp.take(returned, own_slots[:, member], axis=0).astype(jnp.float32)
        combined = combined + own_weights[:, member : member + 1] * chosen
    return combined.astype(jnp.bfloat16)


def solution(mesh):
    return jax.shard_map(
        shards,
        mesh=mesh,
        in_specs=(
            P(("sp", "tp"), None),
            P("sp", "tp"),
            P("sp", "tp"),
            P("sp"),
            P(None, "tp"),
            P("tp"),
            P("tp"),
            P(),
            P(),
            P("sp", None),
            P("sp", None),
            P("sp", None, "tp"),
            P("sp", None, "tp"),
            P("sp", "tp", None),
        ),
        out_specs=P(("sp", "tp"), None),
        check_vma=False,
    )
```

profile of v0, /device:TPU:0, one launch (start us, length us, event | category | flops | bytes accessed | tf_op | source)
XLA Modules:
  0.0 263.9 jit_solution(16011926092684907815)
XLA Ops:
  6.5 0.8 slice.300
  7.3 4.9 %collective-permute-start = (s32[30]{0:T(128)S(1)}, s32[30]{0:T(128)S(1)}, u32[]{:S(2)}, u32[]{:S(2)}) collective-permute-start(s32[30]{0:T(128)S(1)} %slice.300), channel_id=1, source_target_pairs={{0,4},{4,8},{8,12},{12,16},{16,20},{20,24},{24,28},{1,5},{5,9},{9,... | collective-permute-start | bytes 368 | tf_op jit(solution)/shard_map/ppermute | solution.py:13
  12.2 1.2 multiply_convert_fusion.4
  13.4 3.5 %collective-permute-start.1 = (bf16[30,256]{1,0:T(8,128)(2,1)S(1)}, bf16[30,256]{1,0:T(8,128)(2,1)S(1)}, u32[]{:S(2)}, u32[]{:S(2)}) collective-permute-start(bf16[30,256]{1,0:T(8,128)(2,1)S(1)} %slice.404), channel_id=1, source_target_pairs={{0,4},{4,8},{8,12},{12,16},{16,20},{20,24},{24,28},{1,5},{5,9},{9,... | collective-permute-start | bytes 46088 | tf_op jit(solution)/shard_map/ppermute | solution.py:13
  16.8 1.0 fusion.89
  17.9 1.0 fusion.90
  18.9 0.8 pad_add_fusion
  19.6 0.8 slice_compare_fusion.29
  20.4 0.8 slice_compare_fusion.28
  21.2 0.1 maximum_convert_fusion
  21.2 4.0 %fusion.17 = f32[512,256]{1,0:T(8,128)S(1)} fusion(f32[542,256]{1,0:T(8,128)S(1)} %maximum_convert_fusion, f32[256]{0:T(256)S(1)} %bitcast.119, f32[256]{0:T(256)S(1)} %bitcast.120, f32[256]{0:T(256)S(1)} %bitcast.91, f32[256]{0:T(256)S(1)} %bitcast.92, f32[256]{0:T(256)S(1)} %bitcast.93, f32[256]{0:T(256)S(1)} %bitcast.94, f32[256]{0:T(256)S(1)} %bitcast.95, ...), kind=kLoop, calls=%fused_computation.22 | loop fusion | flops 11927552 | bytes 16824320 | tf_op jit(solution)/shard_map/add | solution.py:63
  25.3 0.3 reshape.106
  25.6 0.6 reduce_sum.38
  26.2 1.6 multiply_reduce_fusion.1
  27.9 0.6 mul.495
  28.5 0.6 sub.20
  29.1 4.0 %fusion.11 = f32[512,2048]{1,0:T(8,128)} fusion(bf16[1024,2048]{1,0:T(8,128)(2,1)} %param.23, s32[]{:T(128)S(6)} %select_n.136, f32[64,8,2,128]{3,2,1,0:T(2,128)S(1)} %bitcast.85, f32[512,256]{1,0:T(8,128)S(1)} %fusion.17, f32[64,8,2,128]{3,2,1,0:T(2,128)S(1)} %bitcast.86, f32[256]{0:T(256)S(1)} %copy-done.3, f32[256]{0:T(256)S(1)} %copy-done.4), kind=kOutput, calls=%fused_computation.15 | convolution fusion | flops 538050560 | bytes 6817796 | tf_op jit(solution)/shard_map/dot_general | solution.py:79
  33.1 0.0 all-gather.7.cloned.1.call-start
  33.2 0.7 all-gather.7.cloned.1.call-update
  33.9 0.7 all-gather.11.cloned.1.call-update
  34.7 0.5 all-gather.9.cloned.1.call-update
  35.2 0.1 copy.20
  35.4 0.1 eq.163
  35.5 0.1 eq.159
  35.7 0.6 reduce-window.6
  36.2 0.2 slice_reduce_fusion.2
  36.5 0.1 fusion.84
  36.6 0.1 reduce_sum.41
  36.8 0.1 copy.19
  36.8 0.1 fusion.79
  36.9 41.2 %reduce-scatter.2.cloned.1.call-done = f32[128,2048]{1,0:T(8,128)} async-done(((f32[512,2048]{1,0:T(8,128)}), f32[128,2048]{1,0:T(8,128)}) %reduce-scatter.2.cloned.1.call-update) | async-done | bytes 1048592 | tf_op jit(solution)/shard_map/reduce_scatter | solution.py:78
  78.1 1.3 convert_element_type.59
  79.4 0.3 multiply_reduce_fusion
  79.7 2.2 convolution_convert_fusion
  81.8 5.5 %all-to-all-start = ((bf16[8,64,2048]{2,1,0:T(8,128)(2,1)}), bf16[8,64,2048]{2,1,0:T(8,128)(2,1)S(1)}, u32[]{:S(2)}, u32[]{:S(2)}) async-start(bf16[8,64,2048]{2,1,0:T(8,128)(2,1)} %bitcast.34), calls=%async_computation.1 | async-start | bytes 4194304 | tf_op jit(solution)/shard_map/all_to_all | solution.py:103
  87.3 27.3 %all-gather.7.cloned.1.call-done = bf16[1,2048,1024]{2,1,0:T(8,128)(2,1)} async-done(((bf16[1,2048,256]{2,1,0:T(8,128)(2,1)}), bf16[1,2048,1024]{2,1,0:T(8,128)(2,1)}) %all-gather.7.cloned.1.call-update) | async-done | bytes 4194320 | tf_op jit(solution)/shard_map/all_gather | solution.py:48
  114.7 20.7 %all-to-all-done = bf16[8,64,2048]{2,1,0:T(8,128)(2,1)S(1)} async-done(((bf16[8,64,2048]{2,1,0:T(8,128)(2,1)}), bf16[8,64,2048]{2,1,0:T(8,128)(2,1)S(1)}, u32[]{:S(2)}, u32[]{:S(2)}) %all-to-all-start) | async-done | bytes 2097184 | tf_op jit(solution)/shard_map/all_to_all | solution.py:103
  135.4 6.0 %fusion.4 = f32[512,1024]{1,0:T(8,128)} fusion(bf16[512,2048]{1,0:T(8,128)(2,1)S(1)} %bitcast.88, bf16[1,2048,1024]{2,1,0:T(8,128)(2,1)} %all-gather.7.cloned.1.call-done), kind=kOutput, calls=%fused_computation.6 | convolution fusion | flops 2147483648 | bytes 8388608 | tf_op jit(solution)/shard_map/dot_general | solution.py:106
  141.4 9.4 %all-gather.11.cloned.1.call-done = bf16[1,1024,2048]{2,1,0:T(8,128)(2,1)} async-done(((bf16[1,256,2048]{2,1,0:T(8,128)(2,1)}), bf16[1,1024,2048]{2,1,0:T(8,128)(2,1)}) %all-gather.11.cloned.1.call-update) | async-done | bytes 4194320 | tf_op jit(solution)/shard_map/all_gather | solution.py:51
  150.8 36.4 %all-gather.9.cloned.1.call-done = bf16[1,2048,1024]{2,1,0:T(8,128)(2,1)} async-done(((bf16[1,2048,256]{2,1,0:T(8,128)(2,1)}), bf16[1,2048,1024]{2,1,0:T(8,128)(2,1)}) %all-gather.9.cloned.1.call-update) | async-done | bytes 4194320 | tf_op jit(solution)/shard_map/all_gather | solution.py:49
  187.2 10.0 %fusion.6 = bf16[512,2048]{1,0:T(8,128)(2,1)} fusion(bf16[1,1024,2048]{2,1,0:T(8,128)(2,1)} %all-gather.11.cloned.1.call-done, f32[512,1024]{1,0:T(8,128)} %fusion.4, bf16[512,2048]{1,0:T(8,128)(2,1)S(1)} %bitcast.89, bf16[1,2048,1024]{2,1,0:T(8,128)(2,1)} %all-gather.9.cloned.1.call-done), kind=kOutput, calls=%fused_computation.8 | convolution fusion | flops 4299161600 | bytes 14680064 | tf_op jit(solution)/shard_map/dot_general | solution.py:109
  197.2 5.5 %all-to-all-start.1 = ((bf16[8,64,2048]{2,1,0:T(8,128)(2,1)}), bf16[8,64,2048]{2,1,0:T(8,128)(2,1)S(1)}, u32[]{:S(2)}, u32[]{:S(2)}) async-start(bf16[8,64,2048]{2,1,0:T(8,128)(2,1)} %bitcast.87), calls=%async_computation.2 | async-start | bytes 4194304 | tf_op jit(solution)/shard_map/all_to_all | solution.py:111
  202.8 0.7 constant_dynamic-slice_fusion.1
  203.4 0.2 slice_reduce_fusion.1
  203.7 47.7 %all-to-all-done.1 = bf16[8,64,2048]{2,1,0:T(8,128)(2,1)S(1)} async-done(((bf16[8,64,2048]{2,1,0:T(8,128)(2,1)}), bf16[8,64,2048]{2,1,0:T(8,128)(2,1)S(1)}, u32[]{:S(2)}, u32[]{:S(2)}) %all-to-all-start.1) | async-done | bytes 2097184 | tf_op jit(solution)/shard_map/all_to_all | solution.py:111
  251.4 1.7 gather_fusion
  253.1 1.7 gather_fusion.1
  254.8 2.5 add_convert_fusion
  (30 shorter events, 0.3 us)
Async XLA Ops:
  6.5 28.7 %copy-start = (s32[512,2]{0,1:T(2,128)S(1)}, s32[512,2]{0,1:T(2,128)}, u32[]{:S(2)}) copy-start(s32[512,2]{0,1:T(2,128)} %param.25) | copy-start | bytes 12292
  6.5 71.6 %reduce-scatter.2.cloned.1.call-start = ((), (), s32[]{:S(2)}) async-start(), calls=%async_computation.3 | async-start | bytes 5242880 | tf_op jit(solution)/shard_map/reduce_scatter | solution.py:78
  7.3 11.5 %collective-permute-start = (s32[30]{0:T(128)S(1)}, s32[30]{0:T(128)S(1)}, u32[]{:S(2)}, u32[]{:S(2)}) collective-permute-start(s32[30]{0:T(128)S(1)} %slice.300), channel_id=1, source_target_pairs={{0,4},{4,8},{8,12},{12,16},{16,20},{20,24},{24,28},{1,5},{5,9},{9,... | collective-permute-start | bytes 368 | tf_op jit(solution)/shard_map/ppermute | solution.py:13
  13.4 7.8 %collective-permute-start.1 = (bf16[30,256]{1,0:T(8,128)(2,1)S(1)}, bf16[30,256]{1,0:T(8,128)(2,1)S(1)}, u32[]{:S(2)}, u32[]{:S(2)}) collective-permute-start(bf16[30,256]{1,0:T(8,128)(2,1)S(1)} %slice.404), channel_id=1, source_target_pairs={{0,4},{4,8},{8,12},{12,16},{16,20},{20,24},{24,28},{1,5},{5,9},{9,... | collective-permute-start | bytes 46088 | tf_op jit(solution)/shard_map/ppermute | solution.py:13
  25.6 3.5 %copy-start.3 = (f32[256]{0:T(256)S(1)}, f32[256]{0:T(256)}, u32[]{:S(2)}) copy-start(f32[256]{0:T(256)} %param.22) | copy-start | bytes 3076
  25.6 3.5 %copy-start.4 = (f32[256]{0:T(256)S(1)}, f32[256]{0:T(256)}, u32[]{:S(2)}) copy-start(f32[256]{0:T(256)} %param.21) | copy-start | bytes 3076
  33.1 81.6 %all-gather.7.cloned.1.call-start = ((), (), s32[]{:S(2)}) async-start(), calls=%async_computation.4 | async-start | bytes 5242880 | tf_op jit(solution)/shard_map/all_gather | solution.py:48
  33.9 45.5 %copy-start.1 = (bf16[128,2048]{1,0:T(8,128)(2,1)S(1)}, bf16[128,2048]{1,0:T(8,128)(2,1)}, u32[]{:S(2)}) copy-start(bf16[128,2048]{1,0:T(8,128)(2,1)} %param.16) | copy-start | bytes 1572868
  33.9 116.9 %all-gather.11.cloned.1.call-start = ((), (), s32[]{:S(2)}) async-start(), calls=%async_computation.6 | async-start | bytes 5242880 | tf_op jit(solution)/shard_map/all_gather | solution.py:51
  34.6 45.0 %copy-start.2 = (f32[2048]{0:T(1024)S(1)}, f32[2048]{0:T(1024)}, u32[]{:S(2)}) copy-start(f32[2048]{0:T(1024)} %param.24) | copy-start | bytes 24580
  34.6 152.6 %all-gather.9.cloned.1.call-start = ((), (), s32[]{:S(2)}) async-start(), calls=%async_computation.5 | async-start | bytes 5242880 | tf_op jit(solution)/shard_map/all_gather | solution.py:49
  81.8 53.6 %all-to-all-start = ((bf16[8,64,2048]{2,1,0:T(8,128)(2,1)}), bf16[8,64,2048]{2,1,0:T(8,128)(2,1)S(1)}, u32[]{:S(2)}, u32[]{:S(2)}) async-start(bf16[8,64,2048]{2,1,0:T(8,128)(2,1)} %bitcast.34), calls=%async_computation.1 | async-start | bytes 4194304 | tf_op jit(solution)/shard_map/all_to_all | solution.py:103
  197.2 54.2 %all-to-all-start.1 = ((bf16[8,64,2048]{2,1,0:T(8,128)(2,1)}), bf16[8,64,2048]{2,1,0:T(8,128)(2,1)S(1)}, u32[]{:S(2)}, u32[]{:S(2)}) async-start(bf16[8,64,2048]{2,1,0:T(8,128)(2,1)} %bitcast.87), calls=%async_computation.2 | async-start | bytes 4194304 | tf_op jit(solution)/shard_map/all_to_all | solution.py:111
Sparse Core Ops, SparseCore 0:
  33.2 44.8 reduce-scatter.1
  79.7 34.9 all-gather.6
  116.3 34.4 all-gather.10
  152.2 34.9 all-gather.8
where the time goes:
time: 265 us; the launch traced here: 264 us
  waiting for transfers between devices  185 us (70%)
  matrix products  22.1 us (8%)
  starting transfers between devices  19.5 us (7%)
  other arithmetic  14.7 us (6%)
  between operations  13.4 us (5%)
  local copies, waits for them, and re-layouts  9.39 us (4%)
    all_to_all x1, waiting for transfers between devices, shards(): lax.all_to_all(expert_out, 'sp', split_axis=0, concat_axis=0, tiled=True)  47.7 us
    reduce_scatter x1, waiting for transfers between devices, shards(): lax.psum_scatter(jnp.dot(conv_out, weight_rows, preferred_element_type=jn...  41.2 us
    all_gather x1, waiting for transfers between devices, shards(): lax.all_gather(w_up[0], 'tp', axis=1, tiled=True)  36.4 us
    all_gather x1, waiting for transfers between devices, shards(): lax.all_gather(w_gate[0], 'tp', axis=1, tiled=True)  27.3 us
    all_to_all x1, waiting for transfers between devices, shards(): lax.all_to_all(outgoing, 'sp', split_axis=0, concat_axis=1, tiled=True)  20.7 us
    dot_general x1, matrix products, shards(): summed = jnp.dot(hidden, whole_down, preferred_element_type=jnp.float32)  10 us
    all_gather x1, waiting for transfers between devices, shards(): whole_down = lax.all_gather(w_down[0], 'tp', axis=0, tiled=True)  9.38 us
    ppermute x2, starting transfers between devices, passed_along(): lax.ppermute(value, axis, [(source, source + steps) for source in range(i...  8.32 us
  transfers between devices with their start and end apart: 8, of which 6 were waited for; matrix products, arithmetic and copies ran while one was open for 7% of the time, Pallas kernels for 0%

commit v1 on v0

--- a/solution.py
+++ b/solution.py
@@ -74,13 +74,8 @@
     columns = lax.axis_size("tp")
     column = lax.axis_index("tp")
     rows_own = tok_dev // columns
-    weight_rows = lax.dynamic_slice_in_dim(out_weight, column * local_channels, local_channels, 0)
-    mixed = lax.psum_scatter(
-        jnp.dot(conv_out, weight_rows, preferred_element_type=jnp.float32),
-        "tp",
-        scatter_dimension=0,
-        tiled=True,
-    )
+    own_conv = lax.all_to_all(conv_out, "tp", split_axis=0, concat_axis=1, tiled=True)
+    mixed = jnp.dot(own_conv, out_weight, preferred_element_type=jnp.float32)
     stream = residual.astype(jnp.float32) + lax.optimization_barrier(
         mixed.astype(jnp.bfloat16)
     ).astype(jnp.float32)

time: 265 us -> 199 us (0.75)
  waiting for transfers between devices: 185 us -> 72 us
  blocking collectives: 0 us -> 54 us
    all_to_all x0 -> x1, blocking collectives: none -> 54 us  [shards(): lax.all_to_all(outgoing, 'sp', split_axis=0, concat_axis=1, tiled=True)]
    reduce_scatter x1 -> x0, waiting for transfers between devices: 41.2 us -> none  [shards(): lax.psum_scatter(jnp.dot(conv_out, weight_rows, preferred_element_type=jn...]
    all_gather x1, waiting for transfers between devices: 27.3 us -> 0.01 us  [shards(): lax.all_gather(w_gate[0], 'tp', axis=1, tiled=True)]
    all_gather x1, waiting for transfers between devices: 36.4 us -> 13.8 us  [shards(): lax.all_gather(w_up[0], 'tp', axis=1, tiled=True)]
    all_to_all x1, waiting for transfers between devices: 20.7 us -> 9.03 us  [shards(): lax.all_to_all(conv_out, 'tp', split_axis=0, concat_axis=1, tiled=True)]
    all_gather x1, waiting for transfers between devices: 9.38 us -> 0.01 us  [shards(): whole_down = lax.all_gather(w_down[0], 'tp', axis=0, tiled=True)]
    convert_element_type x1, other arithmetic: 1.28 us -> 4.99 us  [shards(): conv_out = jax.nn.silu(scaled).astype(jnp.bfloat16)]
  transfers between devices with their start and end apart: 8 -> 7, of which waited for: 6 -> 3; matrix products, arithmetic and copies ran while one was open for 7% -> 13% of each run, Pallas kernels for 0% -> 0%
where the time goes in v1:
time: 199 us
  waiting for transfers between devices  72 us (36%)
  blocking collectives  54 us (27%)
  matrix products  19.7 us (10%)
  starting transfers between devices  17.3 us (9%)
  other arithmetic  15.3 us (8%)
  between operations  13.5 us (7%)
  local copies, waits for them, and re-layouts  6.92 us (3%)
    all_to_all x1, blocking collectives, shards(): lax.all_to_all(outgoing, 'sp', split_axis=0, concat_axis=1, tiled=True)  54 us
    all_to_all x1, waiting for transfers between devices, shards(): lax.all_to_all(expert_out, 'sp', split_axis=0, concat_axis=0, tiled=True)  47.7 us
    all_gather x1, waiting for transfers between devices, shards(): lax.all_gather(w_up[0], 'tp', axis=1, tiled=True)  13.8 us
    dot_general x1, matrix products, shards(): summed = jnp.dot(hidden, whole_down, preferred_element_type=jnp.float32)  10 us
    all_to_all x1, waiting for transfers between devices, shards(): lax.all_to_all(conv_out, 'tp', split_axis=0, concat_axis=1, tiled=True)  9.03 us
    ppermute x2, starting transfers between devices, passed_along(): lax.ppermute(value, axis, [(source, source + steps) for source in range(i...  8.32 us
    dot_general x1, matrix products, shards(): gate_act = jnp.dot(arrived, whole_gate, preferred_element_type=jnp.float32)  5.89 us
    all_to_all x1, starting transfers between devices, shards(): lax.all_to_all(expert_out, 'sp', split_axis=0, concat_axis=0, tiled=True)  5.51 us
  transfers between devices with their start and end apart: 7, of which 3 were waited for; matrix products, arithmetic and copies ran while one was open for 13% of the time, Pallas kernels for 0%

profile of v1, /device:TPU:0, one launch (start us, length us, event | category | flops | bytes accessed | tf_op | source)
XLA Modules:
  0.0 198.8 jit_solution(16494497963675948296)
XLA Ops:
  6.5 0.0 all-gather.7.cloned.1.call-start
  6.6 0.7 all-gather.7.cloned.1.call-update
  7.3 0.0 all-gather.11.cloned.1.call-start
  7.3 0.7 all-gather.11.cloned.1.call-update
  8.0 0.0 all-gather.9.cloned.1.call-start
  8.1 0.1 slice.300
  8.2 4.9 %collective-permute-start = (s32[30]{0:T(128)S(1)}, s32[30]{0:T(128)S(1)}, u32[]{:S(2)}, u32[]{:S(2)}) collective-permute-start(s32[30]{0:T(128)S(1)} %slice.300), channel_id=1, source_target_pairs={{0,4},{4,8},{8,12},{12,16},{16,20},{20,24},{24,28},{1,5},{5,9},{9,... | collective-permute-start | bytes 368 | tf_op jit(solution)/shard_map/ppermute | solution.py:13
  13.0 0.2 multiply_convert_fusion.4
  13.2 3.5 %collective-permute-start.1 = (bf16[30,256]{1,0:T(8,128)(2,1)S(1)}, bf16[30,256]{1,0:T(8,128)(2,1)S(1)}, u32[]{:S(2)}, u32[]{:S(2)}) collective-permute-start(bf16[30,256]{1,0:T(8,128)(2,1)S(1)} %slice.404), channel_id=1, source_target_pairs={{0,4},{4,8},{8,12},{12,16},{16,20},{20,24},{24,28},{1,5},{5,9},{9,... | collective-permute-start | bytes 46088 | tf_op jit(solution)/shard_map/ppermute | solution.py:13
  16.7 0.0 all-gather.9.cloned.1.call-update
  16.8 0.1 copy.22
  16.9 0.1 eq.163
  17.1 0.1 eq.159
  17.2 0.6 reduce-window.6
  17.8 0.2 slice_reduce_fusion.2
  18.1 0.1 fusion.79
  18.1 0.1 reduce_sum.41
  18.3 0.1 pad_add_fusion
  18.4 0.1 slice_compare_fusion.29
  18.5 0.1 slice_compare_fusion.28
  18.6 0.1 maximum_convert_fusion
  18.6 4.0 %fusion.15 = f32[512,256]{1,0:T(8,128)S(1)} fusion(f32[542,256]{1,0:T(8,128)S(1)} %maximum_convert_fusion, f32[256]{0:T(256)S(1)} %bitcast.154, f32[256]{0:T(256)S(1)} %bitcast.156, f32[256]{0:T(256)S(1)} %bitcast.98, f32[256]{0:T(256)S(1)} %bitcast.100, f32[256]{0:T(256)S(1)} %bitcast.102, f32[256]{0:T(256)S(1)} %bitcast.104, f32[256]{0:T(256)S(1)} %bitcast.106, ...), kind=kLoop, calls=%fused_computation.21 | loop fusion | flops 11927552 | bytes 16824320 | tf_op jit(solution)/shard_map/add | solution.py:63
  22.7 0.3 reshape.109
  23.0 0.0 copy-start.7
  23.0 0.6 reduce_sum.38
  23.6 1.6 multiply_reduce_fusion.1
  25.3 0.6 mul.492
  25.9 0.6 sub.20
  26.5 5.0 %multiply_convert_fusion.3 = bf16[512,256]{1,0:T(8,128)(2,1)} fusion(f32[64,8,2,128]{3,2,1,0:T(2,128)S(1)} %bitcast.89, f32[64,8,2,128]{3,2,1,0:T(2,128)S(1)} %bitcast.90, f32[256]{0:T(256)S(1)} %copy-done.7, f32[256]{0:T(256)S(1)} %copy-done.8, f32[256]{0:T(256)S(1)} %bitcast.155, f32[542,256]{1,0:T(8,128)S(1)} %maximum_convert_fusion, ...), kind=kLoop, calls=%fused_computation.114 | loop fusion | flops 13107200 | bytes 17612800 | tf_op jit(solution)/shard_map/convert_element_type | solution.py:73
  31.5 3.4 %all-to-all-start = ((bf16[4,128,256]{2,1,0:T(8,128)(2,1)}), bf16[4,128,256]{2,1,0:T(8,128)(2,1)S(1)}, u32[]{:S(2)}, u32[]{:S(2)}) async-start(bf16[4,128,256]{2,1,0:T(8,128)(2,1)} %bitcast.31), calls=%async_computation | async-start | bytes 524288 | tf_op jit(solution)/shard_map/all_to_all | solution.py:77
  34.9 0.1 copy.21
  35.0 0.1 fusion.77
  35.1 9.0 %all-to-all-done = bf16[4,128,256]{2,1,0:T(8,128)(2,1)S(1)} async-done(((bf16[4,128,256]{2,1,0:T(8,128)(2,1)}), bf16[4,128,256]{2,1,0:T(8,128)(2,1)S(1)}, u32[]{:S(2)}, u32[]{:S(2)}) %all-to-all-start) | async-done | bytes 262176 | tf_op jit(solution)/shard_map/all_to_all | solution.py:77
  44.1 0.2 copy.19
  44.3 3.0 %convolution_convert_fusion.1 = bf16[128,2048]{1,0:T(8,128)(2,1)S(1)} fusion(bf16[128,1024]{0,1:T(8,128)(2,1)S(1)} %bitcast.94, bf16[1024,2048]{1,0:T(8,128)(2,1)} %param.23), kind=kOutput, calls=%fused_computation.10 | convolution fusion | flops 537133056 | bytes 4980736 | tf_op jit(solution)/shard_map/dot_general | solution.py:78
  47.3 0.3 multiply_reduce_fusion
  47.6 0.8 convolution_convert_fusion
  48.4 54.0 %all_to_all.33 = bf16[8,64,2048]{2,1,0:T(8,128)(2,1)S(1)} all-to-all(bf16[8,64,2048]{2,1,0:T(8,128)(2,1)S(1)} %bitcast.88), channel_id=1, replica_groups=mesh['sp'=8,'tp'=4] {'sp'}, dimensions={0} | all-to-all | bytes 4194304 | tf_op jit(solution)/shard_map/all_to_all | solution.py:98
  102.4 5.9 %fusion.4 = f32[512,1024]{1,0:T(8,128)} fusion(bf16[512,2048]{1,0:T(8,128)(2,1)S(1)} %bitcast.92, bf16[1,2048,1024]{2,1,0:T(8,128)(2,1)} %all-gather.7.cloned.1.call-done), kind=kOutput, calls=%fused_computation.6 | convolution fusion | flops 2147483648 | bytes 8388608 | tf_op jit(solution)/shard_map/dot_general | solution.py:101
  108.3 13.8 %all-gather.9.cloned.1.call-done = bf16[1,2048,1024]{2,1,0:T(8,128)(2,1)} async-done(((bf16[1,2048,256]{2,1,0:T(8,128)(2,1)}), bf16[1,2048,1024]{2,1,0:T(8,128)(2,1)}) %all-gather.9.cloned.1.call-update) | async-done | bytes 4194320 | tf_op jit(solution)/shard_map/all_gather | solution.py:49
  122.1 10.0 %fusion.6 = bf16[512,2048]{1,0:T(8,128)(2,1)} fusion(bf16[1,1024,2048]{2,1,0:T(8,128)(2,1)} %all-gather.11.cloned.1.call-done, f32[512,1024]{1,0:T(8,128)} %fusion.4, bf16[512,2048]{1,0:T(8,128)(2,1)S(1)} %bitcast.93, bf16[1,2048,1024]{2,1,0:T(8,128)(2,1)} %all-gather.9.cloned.1.call-done), kind=kOutput, calls=%fused_computation.8 | convolution fusion | flops 4299161600 | bytes 14680064 | tf_op jit(solution)/shard_map/dot_general | solution.py:104
  132.2 5.5 %all-to-all-start.2 = ((bf16[8,64,2048]{2,1,0:T(8,128)(2,1)}), bf16[8,64,2048]{2,1,0:T(8,128)(2,1)S(1)}, u32[]{:S(2)}, u32[]{:S(2)}) async-start(bf16[8,64,2048]{2,1,0:T(8,128)(2,1)} %bitcast.91), calls=%async_computation.2 | async-start | bytes 4194304 | tf_op jit(solution)/shard_map/all_to_all | solution.py:106
  137.7 0.7 constant_dynamic-slice_fusion.1
  138.3 0.2 slice_reduce_fusion.1
  138.6 47.7 %all-to-all-done.2 = bf16[8,64,2048]{2,1,0:T(8,128)(2,1)S(1)} async-done(((bf16[8,64,2048]{2,1,0:T(8,128)(2,1)}), bf16[8,64,2048]{2,1,0:T(8,128)(2,1)S(1)}, u32[]{:S(2)}, u32[]{:S(2)}) %all-to-all-start.2) | async-done | bytes 2097184 | tf_op jit(solution)/shard_map/all_to_all | solution.py:106
  186.3 1.7 gather_fusion
  188.0 1.7 gather_fusion.1
  189.8 2.5 %add_convert_fusion = bf16[128,2048]{1,0:T(8,128)(2,1)} fusion(bf16[128,2048]{1,0:T(8,128)(2,1)S(1)} %convolution_convert_fusion.1, bf16[128,2048]{1,0:T(8,128)(2,1)S(1)} %copy-done.1, bf16[128,2048]{1,0:T(8,128)(2,1)} %gather_fusion.1, bf16[128,2048]{1,0:T(8,128)(2,1)} %gather_fusion, f32[128]{0:T(128)S(1)} %get-tuple-element.70, ...), kind=kLoop, calls=%fused_computation.12 | loop fusion | flops 3145728 | bytes 2622720 | tf_op jit(solution)/shard_map/convert_element_type | solution.py:113
  (37 shorter events, 0.3 us)
Async XLA Ops:
  6.5 10.2 %copy-start = (s32[512,2]{0,1:T(2,128)S(1)}, s32[512,2]{0,1:T(2,128)}, u32[]{:S(2)}) copy-start(s32[512,2]{0,1:T(2,128)} %param.25) | copy-start | bytes 12292
  6.5 1.5 copy-start.5
  6.5 6.5 %copy-start.3 = (bf16[512,256]{1,0:T(8,128)(2,1)S(1)}, bf16[512,256]{1,0:T(8,128)(2,1)}, u32[]{:S(2)}) copy-start(bf16[512,256]{1,0:T(8,128)(2,1)} %param.17) | copy-start | bytes 786436
  6.5 6.5 %copy-start.2 = (bf16[512,256]{1,0:T(8,128)(2,1)S(1)}, bf16[512,256]{1,0:T(8,128)(2,1)}, u32[]{:S(2)}) copy-start(bf16[512,256]{1,0:T(8,128)(2,1)} %param.18) | copy-start | bytes 786436
  6.5 10.2 %copy-start.4 = (f32[31,256]{1,0:T(8,128)S(1)}, f32[31,256]{1,0:T(8,128)}, u32[]{:S(2)}) copy-start(f32[31,256]{1,0:T(8,128)} %param.20) | copy-start | bytes 95236
  6.5 95.9 %all-gather.7.cloned.1.call-start = ((), (), s32[]{:S(2)}) async-start(), calls=%async_computation.3 | async-start | bytes 5242880 | tf_op jit(solution)/shard_map/all_gather | solution.py:48
  7.3 101.0 %all-gather.11.cloned.1.call-start = ((), (), s32[]{:S(2)}) async-start(), calls=%async_computation.5 | async-start | bytes 5242880 | tf_op jit(solution)/shard_map/all_gather | solution.py:51
  8.0 114.1 %all-gather.9.cloned.1.call-start = ((), (), s32[]{:S(2)}) async-start(), calls=%async_computation.4 | async-start | bytes 5242880 | tf_op jit(solution)/shard_map/all_gather | solution.py:49
  8.2 10.1 %collective-permute-start = (s32[30]{0:T(128)S(1)}, s32[30]{0:T(128)S(1)}, u32[]{:S(2)}, u32[]{:S(2)}) collective-permute-start(s32[30]{0:T(128)S(1)} %slice.300), channel_id=1, source_target_pairs={{0,4},{4,8},{8,12},{12,16},{16,20},{20,24},{24,28},{1,5},{5,9},{9,... | collective-permute-start | bytes 368 | tf_op jit(solution)/shard_map/ppermute | solution.py:13
  13.2 5.4 %collective-permute-start.1 = (bf16[30,256]{1,0:T(8,128)(2,1)S(1)}, bf16[30,256]{1,0:T(8,128)(2,1)S(1)}, u32[]{:S(2)}, u32[]{:S(2)}) collective-permute-start(bf16[30,256]{1,0:T(8,128)(2,1)S(1)} %slice.404), channel_id=1, source_target_pairs={{0,4},{4,8},{8,12},{12,16},{16,20},{20,24},{24,28},{1,5},{5,9},{9,... | collective-permute-start | bytes 46088 | tf_op jit(solution)/shard_map/ppermute | solution.py:13
  23.0 3.5 %copy-start.7 = (f32[256]{0:T(256)S(1)}, f32[256]{0:T(256)}, u32[]{:S(2)}) copy-start(f32[256]{0:T(256)} %param.22) | copy-start | bytes 3076
  23.0 3.5 %copy-start.8 = (f32[256]{0:T(256)S(1)}, f32[256]{0:T(256)}, u32[]{:S(2)}) copy-start(f32[256]{0:T(256)} %param.21) | copy-start | bytes 3076
  31.5 12.6 %all-to-all-start = ((bf16[4,128,256]{2,1,0:T(8,128)(2,1)}), bf16[4,128,256]{2,1,0:T(8,128)(2,1)S(1)}, u32[]{:S(2)}, u32[]{:S(2)}) async-start(bf16[4,128,256]{2,1,0:T(8,128)(2,1)} %bitcast.31), calls=%async_computation | async-start | bytes 524288 | tf_op jit(solution)/shard_map/all_to_all | solution.py:77
  44.3 3.0 %copy-start.1 = (bf16[128,2048]{1,0:T(8,128)(2,1)S(1)}, bf16[128,2048]{1,0:T(8,128)(2,1)}, u32[]{:S(2)}) copy-start(bf16[128,2048]{1,0:T(8,128)(2,1)} %param.16) | copy-start | bytes 1572868
  44.3 3.3 %copy-start.6 = (f32[2048]{0:T(1024)S(1)}, f32[2048]{0:T(1024)}, u32[]{:S(2)}) copy-start(f32[2048]{0:T(1024)} %param.24) | copy-start | bytes 24580
  132.2 54.2 %all-to-all-start.2 = ((bf16[8,64,2048]{2,1,0:T(8,128)(2,1)}), bf16[8,64,2048]{2,1,0:T(8,128)(2,1)S(1)}, u32[]{:S(2)}, u32[]{:S(2)}) async-start(bf16[8,64,2048]{2,1,0:T(8,128)(2,1)} %bitcast.91), calls=%async_computation.2 | async-start | bytes 4194304 | tf_op jit(solution)/shard_map/all_to_all | solution.py:106
Sparse Core Ops, SparseCore 0:
  8.9 40.5 all-gather.6
  51.0 34.4 all-gather.10
  87.1 34.9 all-gather.8

commit v2 on v1

--- a/solution.py
+++ b/solution.py
@@ -1,10 +1,16 @@
+import functools
+
 import jax
 import jax.numpy as jnp
 from jax import lax
+from jax.experimental import pallas as pl
+from jax.experimental.pallas import tpu as pltpu
 from jax.sharding import PartitionSpec as P
 
 DC = 1024
 CONV_GROUPS = 8
+MESH = pl.DeviceIdType.MESH
+RIM = 32
 
 
 def passed_along(value, axis, steps):
@@ -26,7 +32,7 @@
     return matches.astype(jnp.bfloat16)
 
 
-def shards(
+def plain_shards(
     residual,
     conv_value,
     conv_gate,
@@ -113,6 +119,300 @@
     return combined.astype(jnp.bfloat16)
 
 
+def flipped(index, mask):
+    bit = 1
+    while bit <= mask:
+        if mask & bit:
+            index = index + bit * (1 - 2 * ((index // bit) % 2))
+        bit *= 2
+    return index
+
+
+def layer_kernel(
+    experts_n, columns, capacity,
+    residual_ref, value_ref, gate_ref, seg_ref, conv_w_ref, gain_ref, shift_ref, ow_hbm, ffn_ref,
+    slots_t_ref, slots_ref, route_w_ref, wg_ref, wu_ref, wd_ref,
+    out_ref,
+    ow, wg_in, wu_in, wd_in, rim, seg_ext, ext, conv_out, conv_in, stream, normed,
+    outgoing, arrived, hidden, results, returned,
+    ow_sem, y_send, y_recv, c_send, c_recv, f_send, f_recv, rim_send, rim_recv,
+    x_send, x_recv, d_send, d_recv, r_send, r_recv,
+):
+    me_s, me_t = lax.axis_index("sp"), lax.axis_index("tp")
+    tok_dev, local = value_ref.shape
+    width = residual_ref.shape[1]
+    rows_own = tok_dev // columns
+    taps = conv_w_ref.shape[0]
+    next_s = (me_s + 1) % experts_n
+    previous_s = (me_s + experts_n - 1) % experts_n
+    tile = 512
+
+    ow_copy = pltpu.make_async_copy(ow_hbm, ow, ow_sem)
+    ow_copy.start()
+
+    def tp_peer(mask):
+        return (me_s, flipped(me_t, mask))
+
+    def sp_peer(mask):
+        return (flipped(me_s, mask), me_t)
+
+    barrier = pltpu.get_barrier_semaphore()
+    peers = [tp_peer(mask) for mask in range(1, columns)]
+    peers += [sp_peer(mask) for mask in range(1, experts_n)]
+    for peer in peers:
+        pl.semaphore_signal(barrier, inc=1, device_id=peer, device_id_type=MESH)
+    pl.semaphore_wait(barrier, len(peers))
+
+    def remote(src, dst, send, recv, peer):
+        return pltpu.make_async_remote_copy(
+            src_ref=src, dst_ref=dst, send_sem=send, recv_sem=recv,
+            device_id=peer, device_id_type=MESH,
+        )
+
+    rim_copies = [
+        remote(ref.at[pl.ds(tok_dev - RIM, RIM)], dst, rim_send.at[i], rim_recv.at[i], (next_s, me_t))
+        for i, (ref, dst) in enumerate(
+            ((value_ref, rim.at[0]), (gate_ref, rim.at[1]), (seg_ref, seg_ext.at[pl.ds(0, RIM)]))
+        )
+    ]
+    for copy in rim_copies:
+        copy.start()
+
+    half = width // 2
+    pieces = (
+        (wg_ref, wg_in, 0, half), (wg_ref, wg_in, half, half),
+        (wu_ref, wu_in, 0, width), (wd_ref, wd_in, 0, local),
+    )
+    across = [
+        remote(own.at[pl.ds(row, n)], into.at[1, pl.ds(row, n)], y_send.at[i], y_recv.at[i], tp_peer(2))
+        for i, (own, into, row, n) in enumerate(pieces)
+    ]
+    forward = [
+        remote(into.at[1, pl.ds(row, n)], into.at[2, pl.ds(row, n)], f_send.at[i], f_recv.at[i], tp_peer(1))
+        for i, (own, into, row, n) in enumerate(pieces)
+    ]
+    beside = [
+        remote(own, into.at[0], c_send.at[i], c_recv.at[i], tp_peer(1))
+        for i, (own, into) in enumerate(((wg_ref, wg_in), (wu_ref, wu_in), (wd_ref, wd_in)))
+    ]
+    across[0].start()
+
+    def gated_of(value, gate):
+        value, gate = value.astype(jnp.float32), gate.astype(jnp.float32)
+        product = value * (1.0 / (1.0 + jnp.exp(-gate)))
+        return product.astype(jnp.bfloat16).astype(jnp.float32)
+
+    def gate_rows(i, carry):
+        row = pl.multiple_of(i * 64, 64)
+        ext[pl.ds(row + RIM, 64), :] = gated_of(value_ref[pl.ds(row, 64), :], gate_ref[pl.ds(row, 64), :])
+        seg_ext[pl.ds(row + RIM, 64), :] = seg_ref[pl.ds(row, 64), :]
+        return carry
+
+    lax.fori_loop(0, tok_dev // 64, gate_rows, 0)
+    for copy in rim_copies:
+        copy.wait_recv()
+    ext[pl.ds(0, RIM), :] = gated_of(rim[0], rim[1])
+    seg_ext[pl.ds(0, RIM), :] = jnp.where(me_s == 0, -1, seg_ext[pl.ds(0, RIM), :])
+
+    group = DC // CONV_GROUPS
+    block = 64
+    lead = RIM - (taps - 1)
+    for row in range(0, tok_dev, block):
+        own_seg = seg_ref[row : row + block, :]
+        sums = [jnp.zeros((block, group), jnp.float32) for _ in range(local // group)]
+        for tap in range(taps):
+            at = row + lead + tap
+            same_doc = seg_ext[at : at + block, :] == own_seg
+            for g in range(local // group):
+                lanes = slice(g * group, (g + 1) * group)
+                term = ext[at : at + block, lanes] * conv_w_ref[tap : tap + 1, lanes]
+                sums[g] = sums[g] + jnp.where(same_doc, term, 0.0)
+        for g in range(local // group):
+            lanes = slice(g * group, (g + 1) * group)
+            mean = jnp.mean(sums[g], axis=-1, keepdims=True)
+            centred = sums[g] - mean
+            deviation = jnp.mean(centred * centred, axis=-1, keepdims=True)
+            scaled = centred * lax.rsqrt(deviation + 1e-05) * gain_ref[:, lanes] + shift_ref[:, lanes]
+            conv_out[row : row + block, lanes] = (scaled / (1.0 + jnp.exp(-scaled))).astype(jnp.bfloat16)
+
+    exchange = {}
+    for mask in (3, 2, 1):
+        peer_rows = pl.ds(pl.multiple_of(flipped(me_t, mask) * rows_own, rows_own), rows_own)
+        exchange[mask] = remote(
+            conv_out.at[peer_rows], conv_in.at[mask], x_send.at[mask], x_recv.at[mask], tp_peer(mask)
+        )
+        exchange[mask].start()
+    for copy in across[1:] + beside:
+        copy.start()
+    conv_in[0] = conv_out[pl.ds(pl.multiple_of(me_t * rows_own, rows_own), rows_own), :]
+    ow_copy.wait()
+    for mask in (1, 2, 3):
+        exchange[mask].wait_recv()
+
+    squares = jnp.zeros((rows_own, 1), jnp.float32)
+    for col in range(0, width, tile):
+        cols = slice(col, col + tile)
+        mixed = jnp.zeros((rows_own, tile), jnp.float32)
+        for mask in range(columns):
+            w_rows = pl.ds(pl.multiple_of(flipped(me_t, mask) * local, local), local)
+            mixed = mixed + jnp.dot(conv_in[mask], ow[w_rows, cols], preferred_element_type=jnp.float32)
+        part = residual_ref[:, cols].astype(jnp.float32) + mixed.astype(jnp.bfloat16).astype(jnp.float32)
+        stream[:, cols] = part
+        squares = squares + jnp.sum(part * part, axis=-1, keepdims=True)
+    scale = lax.rsqrt(squares / width + 1e-06)
+    normed[...] = (stream[...] * scale * ffn_ref[...]).astype(jnp.bfloat16)
+
+    dispatch = [
+        None if mask == 0 else remote(
+            outgoing.at[pl.ds(mask * capacity, capacity)], arrived.at[pl.ds(mask * capacity, capacity)],
+            d_send.at[mask], d_recv.at[mask], sp_peer(mask),
+        )
+        for mask in range(experts_n)
+    ]
+    half_slots = experts_n * capacity // 2
+    for part in (1, 0):
+        first = part * half_slots
+        numbers = lax.broadcasted_iota(jnp.int32, (half_slots, rows_own), 0) + first
+        picks = jnp.where(numbers == slots_t_ref[0:1, :], 1.0, 0.0)
+        for member in range(1, slots_t_ref.shape[0]):
+            picks = picks + jnp.where(numbers == slots_t_ref[member : member + 1, :], 1.0, 0.0)
+        picks = picks.astype(jnp.bfloat16)
+        for col in range(0, width, tile):
+            cols = slice(col, col + tile)
+            outgoing[first : first + half_slots, cols] = jnp.dot(
+                picks, normed[:, cols], preferred_element_type=jnp.float32
+            ).astype(jnp.bfloat16)
+        for mask in reversed(range(part * experts_n // 2, (part + 1) * experts_n // 2)):
+            if mask:
+                dispatch[mask].start()
+    arrived[0:capacity, :] = outgoing[0:capacity, :]
+
+    near, far = slice(0, half_slots), slice(half_slots, 2 * half_slots)
+
+    def hidden_units(mask, rows):
+        g = wg_ref[...] if mask == 0 else wg_in[mask - 1]
+        u = wu_ref[...] if mask == 0 else wu_in[mask - 1]
+        gate_act = jnp.dot(arrived[rows, :], g, preferred_element_type=jnp.float32)
+        up_act = jnp.dot(arrived[rows, :], u, preferred_element_type=jnp.float32)
+        hidden[mask, rows, :] = (gate_act / (1.0 + jnp.exp(-gate_act)) * up_act).astype(jnp.bfloat16)
+
+    for copy in beside:
+        copy.wait_recv()
+    for i in (0, 1):
+        across[i].wait_recv()
+        forward[i].start()
+    for mask in range(1, experts_n // 2):
+        dispatch[mask].wait_recv()
+    hidden_units(0, near)
+    hidden_units(1, near)
+    across[2].wait_recv()
+    forward[2].start()
+    hidden_units(2, near)
+    for i in (0, 1, 2):
+        forward[i].wait_recv()
+    hidden_units(3, near)
+    for mask in range(experts_n // 2, experts_n):
+        dispatch[mask].wait_recv()
+    for mask in range(columns):
+        hidden_units(mask, far)
+    across[3].wait_recv()
+    forward[3].start()
+    forward[3].wait_recv()
+
+    give_back = [
+        None if mask == 0 else remote(
+            results.at[pl.ds(mask * capacity, capacity)], returned.at[pl.ds(mask * capacity, capacity)],
+            r_send.at[mask], r_recv.at[mask], sp_peer(mask),
+        )
+        for mask in range(experts_n)
+    ]
+    for part in (1, 0):
+        rows = (near, far)[part]
+        for col in range(0, width, tile):
+            cols = slice(col, col + tile)
+            total = jnp.dot(hidden[0, rows, :], wd_ref[:, cols], preferred_element_type=jnp.float32)
+            for mask in range(1, columns):
+                total = total + jnp.dot(
+                    hidden[mask, rows, :], wd_in[mask - 1, :, cols], preferred_element_type=jnp.float32
+                )
+            results[rows, cols] = total.astype(jnp.bfloat16)
+        for mask in reversed(range(part * experts_n // 2, (part + 1) * experts_n // 2)):
+            if mask:
+                give_back[mask].start()
+    returned[0:capacity, :] = results[0:capacity, :]
+
+    for mask in range(1, experts_n):
+        give_back[mask].wait_recv()
+    places = lax.broadcasted_iota(jnp.int32, (rows_own, experts_n * capacity), 1)
+    tables = [
+        jnp.where(places == slots_ref[:, m : m + 1], 1.0, 0.0).astype(jnp.bfloat16)
+        for m in range(slots_ref.shape[1])
+    ]
+    for col in range(0, width, tile):
+        cols = slice(col, col + tile)
+        total = stream[:, cols]
+        for m, table in enumerate(tables):
+            chosen = jnp.dot(table, returned[:, cols], preferred_element_type=jnp.float32)
+            total = total + route_w_ref[:, m : m + 1] * chosen
+        out_ref[:, cols] = total.astype(jnp.bfloat16)
+
+    for copy in rim_copies + across + forward + beside + list(exchange.values()):
+        copy.wait_send()
+    for mask in range(1, experts_n):
+        dispatch[mask].wait_send()
+        give_back[mask].wait_send()
+
+
+def shards(*args):
+    (residual, conv_value, conv_gate, segments, conv_weight, norm_gain, norm_shift, out_weight,
+     ffn_gain, routes, route_weights, w_gate, w_up, w_down) = args
+    tok_dev, local = conv_value.shape
+    width = residual.shape[1]
+    experts_n, columns = lax.axis_size("sp"), lax.axis_size("tp")
+    top_count = routes.shape[1]
+    capacity = max(2, 2 * tok_dev * top_count // (columns * experts_n))
+    if capacity % 16 or columns != 4 or experts_n & (experts_n - 1):
+        return plain_shards(*args)
+    rows_own = tok_dev // columns
+    first = lax.axis_index("tp") * rows_own
+    own_routes = lax.dynamic_slice_in_dim(routes, first, rows_own, 0) ^ lax.axis_index("sp")
+    own_weights = lax.dynamic_slice_in_dim(route_weights, first, rows_own, 0)
+    slots = slot_numbers(own_routes, capacity, experts_n)
+    lanes = DC // CONV_GROUPS
+    slot_total = experts_n * capacity
+    bf16, f32 = jnp.bfloat16, jnp.float32
+    vmem, dma = pltpu.VMEM, pltpu.SemaphoreType.DMA
+    spec = pl.BlockSpec(memory_space=pltpu.VMEM)
+    specs = [spec] * 15
+    specs[7] = pl.BlockSpec(memory_space=pl.ANY)
+    return pl.pallas_call(
+        functools.partial(layer_kernel, experts_n, columns, capacity),
+        out_shape=jax.ShapeDtypeStruct((rows_own, width), bf16),
+        in_specs=specs,
+        out_specs=spec,
+        scratch_shapes=[
+            vmem(out_weight.shape, bf16),
+            vmem((3, width, local), bf16), vmem((3, width, local), bf16), vmem((3, local, width), bf16),
+            vmem((2, RIM, local), bf16), vmem((RIM + tok_dev, lanes), jnp.int32),
+            vmem((RIM + tok_dev, local), f32), vmem((tok_dev, local), bf16),
+            vmem((columns, rows_own, local), bf16), vmem((rows_own, width), f32),
+            vmem((rows_own, width), bf16), vmem((slot_total, width), bf16),
+            vmem((slot_total, width), bf16), vmem((columns, slot_total, local), bf16),
+            vmem((slot_total, width), bf16), vmem((slot_total, width), bf16),
+            dma, dma((4,)), dma((4,)), dma((3,)), dma((3,)), dma((4,)), dma((4,)), dma((3,)), dma((3,)),
+            dma((4,)), dma((4,)), dma((experts_n,)), dma((experts_n,)), dma((experts_n,)), dma((experts_n,)),
+        ],
+        compiler_params=pltpu.CompilerParams(
+            collective_id=0, has_side_effects=True, vmem_limit_bytes=60 * 1024 * 1024
+        ),
+    )(
+        residual, conv_value, conv_gate,
+        jnp.broadcast_to(segments[:, None], (tok_dev, lanes)), conv_weight,
+        norm_gain[None], norm_shift[None], out_weight, ffn_gain[None],
+        slots.T, slots, own_weights, w_gate[0], w_up[0], w_down[0],
+    )
+
+
 def solution(mesh):
     return jax.shard_map(
         shards,

time: 199 us -> 143 us (0.72)
  Pallas kernels: 0 us -> 135 us
  waiting for transfers between devices: 72 us -> 0 us
  blocking collectives: 54 us -> 0 us
  matrix products: 19.7 us -> 0 us
  starting transfers between devices: 17.3 us -> 0 us
  other arithmetic: 15.3 us -> 0.74 us
  between operations: 13.5 us -> 0.06 us
    pallas_call x0 -> x1, Pallas kernels: none -> 135 us  [shards(): pl.pallas_call(functools.partial(layer_kernel, experts_n, columns, capaci...]
    all_to_all x2 -> x0, waiting for transfers between devices: 56.8 us -> none  [the longest x1 47.7 us: shards(): lax.all_to_all(expert_out, 'sp', split_axis=0, concat_axis=0, tiled=True)]
    all_to_all x1 -> x0, blocking collectives: 54 us -> none  [shards(): lax.all_to_all(outgoing, 'sp', split_axis=0, concat_axis=1, tiled=True)]
    dot_general x4 -> x0, matrix products: 19.7 us -> none  [the longest x1 10 us: shards(): summed = jnp.dot(hidden, whole_down, preferred_element_type=jnp.float32)]
    all_gather x3 -> x0, waiting for transfers between devices: 13.8 us -> none  [the longest x1 13.8 us: shards(): lax.all_gather(w_up[0], 'tp', axis=1, tiled=True)]
    all_to_all x2 -> x0, starting transfers between devices: 8.92 us -> none  [the longest x1 5.51 us: shards(): lax.all_to_all(expert_out, 'sp', split_axis=0, concat_axis=0, tiled=True)]
    ppermute x2 -> x0, starting transfers between devices: 8.32 us -> none  [passed_along(): lax.ppermute(value, axis, [(source, source + steps) for source in range(i...]
    convert_element_type x4 -> x0, other arithmetic: 7.69 us -> none  [the longest x1 4.99 us: shards(): conv_out = jax.nn.silu(scaled).astype(jnp.bfloat16)]
  transfers between devices with their start and end apart: 7 -> 0, of which waited for: 3 -> 0; matrix products, arithmetic and copies ran while one was open for 13% -> 0% of each run, Pallas kernels for 0% -> 0%
where the time goes in v2:
time: 143 us
  Pallas kernels  135 us (94%)
  local copies, waits for them, and re-layouts  6.85 us (5%)
    pallas_call x1, Pallas kernels, shards(): pl.pallas_call(functools.partial(layer_kernel, experts_n, columns, capaci...  135 us
    unnamed x7, local copies, waits for them, and re-layouts  3.41 us

profile of v2, /device:TPU:0, one launch (start us, length us, event | category | flops | bytes accessed | tf_op | source)
XLA Modules:
  0.0 142.9 jit_solution(8973850046085828461)
XLA Ops:
  0.0 0.0 copy-start
  0.0 0.7 copy-done
  0.7 0.7 constant_dynamic-slice_fusion
  1.4 0.1 copy.21
  1.5 0.7 copy.22.route_w_ref
  2.2 0.1 eq.25
  2.4 0.1 eq.29
  2.5 0.6 reduce-window.6
  3.1 0.2 slice_reduce_fusion
  3.4 0.1 fusion.1
  3.5 0.1 reduce_sum.12
  3.6 0.0 copy-start.1
  3.6 0.6 copy.20.slots_t_ref
  4.2 1.5 %broadcast_in_dim.16.seg_ref = s32[512,128]{1,0:T(8,128)} broadcast(s32[512]{0:T(512)} %param.17), dimensions={0} | broadcast | bytes 264192 | tf_op jit(solution)/shard_map/broadcast_in_dim | solution.py:410
  5.8 0.0 copy-done.1
  5.8 135.2 %shard_map.136 = bf16[128,2048]{1,0:T(8,128)(2,1)} custom-call(bf16[128,2048]{1,0:T(8,128)(2,1)} %residual_ref.1, bf16[512,256]{1,0:T(8,128)(2,1)} %value_ref.1, bf16[512,256]{1,0:T(8,128)(2,1)} %gate_ref.1, s32[512,128]{1,0:T(8,128)} %broadcast_in_dim.16.seg_ref, f32[31,256]{1,0:T(8,128)} %conv_w_ref.1, f32[1,256]{1,0:T(1,128)} %bitcast.20, ...), custom_call_target="tpu_custom_call" | custom-call | tf_op jit(solution)/shard_map/pallas_call | solution.py:388
  141.0 1.9 %copy.24 = bf16[128,2048]{1,0:T(8,128)(2,1)} copy(bf16[128,2048]{1,0:T(8,128)(2,1)} %shard_map.136) | data formatting | bytes 1048576
  (6 shorter events, 0.1 us)
Async XLA Ops:
  0.0 0.7 copy-start
  3.6 2.1 %copy-start.1 = (s32[128,2]{1,0:T(8,128)}, s32[128,2]{1,0:T(8,128)S(1)}, u32[]{:S(2)}) copy-start(s32[128,2]{1,0:T(8,128)S(1)} %multiply_add_fusion.slots_ref) | copy-start | bytes 3076

commit v3 on v2

--- a/solution.py
+++ b/solution.py
@@ -131,10 +131,10 @@
 def layer_kernel(
     experts_n, columns, capacity,
     residual_ref, value_ref, gate_ref, seg_ref, conv_w_ref, gain_ref, shift_ref, ow_hbm, ffn_ref,
-    slots_t_ref, slots_ref, route_w_ref, wg_ref, wu_ref, wd_ref,
+    routes_ref, route_w_ref, wg_ref, wu_ref, wd_ref,
     out_ref,
     ow, wg_in, wu_in, wd_in, rim, seg_ext, ext, conv_out, conv_in, stream, normed,
-    outgoing, arrived, hidden, results, returned,
+    outgoing, arrived, hidden, partial, results, returned, seg_in, tables,
     ow_sem, y_send, y_recv, c_send, c_recv, f_send, f_recv, rim_send, rim_recv,
     x_send, x_recv, d_send, d_recv, r_send, r_recv,
 ):
@@ -169,10 +169,11 @@
             device_id=peer, device_id_type=MESH,
         )
 
+    last = pl.ds(tok_dev - RIM, RIM)
     rim_copies = [
-        remote(ref.at[pl.ds(tok_dev - RIM, RIM)], dst, rim_send.at[i], rim_recv.at[i], (next_s, me_t))
+        remote(ref, dst, rim_send.at[i], rim_recv.at[i], (next_s, me_t))
         for i, (ref, dst) in enumerate(
-            ((value_ref, rim.at[0]), (gate_ref, rim.at[1]), (seg_ref, seg_ext.at[pl.ds(0, RIM)]))
+            ((value_ref.at[last], rim.at[0]), (gate_ref.at[last], rim.at[1]), (seg_ref, seg_in))
         )
     ]
     for copy in rim_copies:
@@ -205,20 +206,42 @@
     def gate_rows(i, carry):
         row = pl.multiple_of(i * 64, 64)
         ext[pl.ds(row + RIM, 64), :] = gated_of(value_ref[pl.ds(row, 64), :], gate_ref[pl.ds(row, 64), :])
-        seg_ext[pl.ds(row + RIM, 64), :] = seg_ref[pl.ds(row, 64), :]
         return carry
 
     lax.fori_loop(0, tok_dev // 64, gate_rows, 0)
+    lanes_n = seg_ref.shape[1]
+
+    def column(row):
+        return jnp.broadcast_to(row.astype(jnp.float32), (lanes_n, lanes_n)).T
+
+    for i in range(seg_ref.shape[0]):
+        seg_ext[RIM + i * lanes_n : RIM + (i + 1) * lanes_n, :] = column(seg_ref[i : i + 1, :])
+    own_lanes = pl.ds(pl.multiple_of(me_t * rows_own, rows_own), rows_own)
+    numbers = lax.broadcasted_iota(jnp.int32, (rows_own, lanes_n), 1).astype(jnp.float32)
+    names = [column(routes_ref[m : m + 1, own_lanes]) for m in range(routes_ref.shape[0])]
+    shares = [column(route_w_ref[m : m + 1, own_lanes])[:, 0:1] for m in range(routes_ref.shape[0])]
+    marks = [jnp.where(name == numbers, 1.0, 0.0) for name in names]
+    earlier = jnp.where(
+        lax.broadcasted_iota(jnp.int32, (rows_own, rows_own), 0)
+        > lax.broadcasted_iota(jnp.int32, (rows_own, rows_own), 1), 1.0, 0.0,
+    ).astype(jnp.bfloat16)
+    counts = jnp.dot(earlier, sum(marks).astype(jnp.bfloat16), preferred_element_type=jnp.float32)
+    slot_places = lax.broadcasted_iota(jnp.int32, (rows_own, experts_n * capacity), 1)
+    for m, mark in enumerate(marks):
+        rank = jnp.sum(counts * mark, axis=-1, keepdims=True).astype(jnp.int32)
+        slot = (names[m][:, 0:1].astype(jnp.int32) ^ me_s) * capacity + rank
+        tables[m] = jnp.where(slot_places == slot, 1.0, 0.0).astype(jnp.bfloat16)
     for copy in rim_copies:
         copy.wait_recv()
     ext[pl.ds(0, RIM), :] = gated_of(rim[0], rim[1])
-    seg_ext[pl.ds(0, RIM), :] = jnp.where(me_s == 0, -1, seg_ext[pl.ds(0, RIM), :])
+    before = column(seg_in[seg_ref.shape[0] - 1 : seg_ref.shape[0], :])[lanes_n - RIM :, :]
+    seg_ext[0:RIM, :] = jnp.where(me_s == 0, -1.0, before)
 
     group = DC // CONV_GROUPS
     block = 64
     lead = RIM - (taps - 1)
     for row in range(0, tok_dev, block):
-        own_seg = seg_ref[row : row + block, :]
+        own_seg = seg_ext[row + RIM : row + RIM + block, :]
         sums = [jnp.zeros((block, group), jnp.float32) for _ in range(local // group)]
         for tap in range(taps):
             at = row + lead + tap
@@ -272,11 +295,9 @@
     half_slots = experts_n * capacity // 2
     for part in (1, 0):
         first = part * half_slots
-        numbers = lax.broadcasted_iota(jnp.int32, (half_slots, rows_own), 0) + first
-        picks = jnp.where(numbers == slots_t_ref[0:1, :], 1.0, 0.0)
-        for member in range(1, slots_t_ref.shape[0]):
-            picks = picks + jnp.where(numbers == slots_t_ref[member : member + 1, :], 1.0, 0.0)
-        picks = picks.astype(jnp.bfloat16)
+        picks = sum(
+            tables[m, :, first : first + half_slots].astype(jnp.float32) for m in range(len(names))
+        ).T.astype(jnp.bfloat16)
         for col in range(0, width, tile):
             cols = slice(col, col + tile)
             outgoing[first : first + half_slots, cols] = jnp.dot(
@@ -315,8 +336,19 @@
         dispatch[mask].wait_recv()
     for mask in range(columns):
         hidden_units(mask, far)
+    def down(mask, rows, cols):
+        w = wd_ref[:, cols] if mask == 0 else wd_in[mask - 1, :, cols]
+        return jnp.dot(hidden[mask, rows, :], w, preferred_element_type=jnp.float32)
+
+    for rows in (far, near):
+        for col in range(0, width, tile):
+            cols = slice(col, col + tile)
+            partial[rows, cols] = down(0, rows, cols) + down(1, rows, cols)
     across[3].wait_recv()
     forward[3].start()
+    for col in range(0, width, tile):
+        cols = slice(col, col + tile)
+        partial[far, cols] += down(2, far, cols)
     forward[3].wait_recv()
 
     give_back = [
@@ -330,31 +362,30 @@
         rows = (near, far)[part]
         for col in range(0, width, tile):
             cols = slice(col, col + tile)
-            total = jnp.dot(hidden[0, rows, :], wd_ref[:, cols], preferred_element_type=jnp.float32)
-            for mask in range(1, columns):
-                total = total + jnp.dot(
-                    hidden[mask, rows, :], wd_in[mask - 1, :, cols], preferred_element_type=jnp.float32
-                )
+            total = partial[rows, cols] + down(3, rows, cols)
+            if part == 0:
+                total = total + down(2, rows, cols)
             results[rows, cols] = total.astype(jnp.bfloat16)
         for mask in reversed(range(part * experts_n // 2, (part + 1) * experts_n // 2)):
             if mask:
                 give_back[mask].start()
     returned[0:capacity, :] = results[0:capacity, :]
 
-    for mask in range(1, experts_n):
-        give_back[mask].wait_recv()
-    places = lax.broadcasted_iota(jnp.int32, (rows_own, experts_n * capacity), 1)
-    tables = [
-        jnp.where(places == slots_ref[:, m : m + 1], 1.0, 0.0).astype(jnp.bfloat16)
-        for m in range(slots_ref.shape[1])
-    ]
-    for col in range(0, width, tile):
-        cols = slice(col, col + tile)
-        total = stream[:, cols]
-        for m, table in enumerate(tables):
-            chosen = jnp.dot(table, returned[:, cols], preferred_element_type=jnp.float32)
-            total = total + route_w_ref[:, m : m + 1] * chosen
-        out_ref[:, cols] = total.astype(jnp.bfloat16)
+    for part in (0, 1):
+        rows = (near, far)[part]
+        for mask in range(part * experts_n // 2, (part + 1) * experts_n // 2):
+            if mask:
+                give_back[mask].wait_recv()
+        for col in range(0, width, tile):
+            cols = slice(col, col + tile)
+            total = stream[:, cols]
+            for m, share in enumerate(shares):
+                chosen = jnp.dot(tables[m, :, rows], returned[rows, cols], preferred_element_type=jnp.float32)
+                total = total + share * chosen
+            if part == 0:
+                stream[:, cols] = total
+            else:
+                out_ref[:, cols] = total.astype(jnp.bfloat16)
 
     for copy in rim_copies + across + forward + beside + list(exchange.values()):
         copy.wait_send()
@@ -371,19 +402,15 @@
     experts_n, columns = lax.axis_size("sp"), lax.axis_size("tp")
     top_count = routes.shape[1]
     capacity = max(2, 2 * tok_dev * top_count // (columns * experts_n))
-    if capacity % 16 or columns != 4 or experts_n & (experts_n - 1):
+    if capacity % 32 or columns != 4 or tok_dev != columns * 128 or experts_n & (experts_n - 1):
         return plain_shards(*args)
     rows_own = tok_dev // columns
-    first = lax.axis_index("tp") * rows_own
-    own_routes = lax.dynamic_slice_in_dim(routes, first, rows_own, 0) ^ lax.axis_index("sp")
-    own_weights = lax.dynamic_slice_in_dim(route_weights, first, rows_own, 0)
-    slots = slot_numbers(own_routes, capacity, experts_n)
     lanes = DC // CONV_GROUPS
     slot_total = experts_n * capacity
     bf16, f32 = jnp.bfloat16, jnp.float32
     vmem, dma = pltpu.VMEM, pltpu.SemaphoreType.DMA
     spec = pl.BlockSpec(memory_space=pltpu.VMEM)
-    specs = [spec] * 15
+    specs = [spec] * 14
     specs[7] = pl.BlockSpec(memory_space=pl.ANY)
     return pl.pallas_call(
         functools.partial(layer_kernel, experts_n, columns, capacity),
@@ -393,12 +420,14 @@
         scratch_shapes=[
             vmem(out_weight.shape, bf16),
             vmem((3, width, local), bf16), vmem((3, width, local), bf16), vmem((3, local, width), bf16),
-            vmem((2, RIM, local), bf16), vmem((RIM + tok_dev, lanes), jnp.int32),
+            vmem((2, RIM, local), bf16), vmem((RIM + tok_dev, lanes), f32),
             vmem((RIM + tok_dev, local), f32), vmem((tok_dev, local), bf16),
             vmem((columns, rows_own, local), bf16), vmem((rows_own, width), f32),
             vmem((rows_own, width), bf16), vmem((slot_total, width), bf16),
             vmem((slot_total, width), bf16), vmem((columns, slot_total, local), bf16),
+            vmem((slot_total, width), f32),
             vmem((slot_total, width), bf16), vmem((slot_total, width), bf16),
+            vmem((tok_dev // lanes, lanes), jnp.int32), vmem((top_count, rows_own, slot_total), bf16),
             dma, dma((4,)), dma((4,)), dma((3,)), dma((3,)), dma((4,)), dma((4,)), dma((3,)), dma((3,)),
             dma((4,)), dma((4,)), dma((experts_n,)), dma((experts_n,)), dma((experts_n,)), dma((experts_n,)),
         ],
@@ -407,9 +436,9 @@
         ),
     )(
         residual, conv_value, conv_gate,
-        jnp.broadcast_to(segments[:, None], (tok_dev, lanes)), conv_weight,
+        segments.reshape(-1, lanes), conv_weight,
         norm_gain[None], norm_shift[None], out_weight, ffn_gain[None],
-        slots.T, slots, own_weights, w_gate[0], w_up[0], w_down[0],
+        routes.T, route_weights.T, w_gate[0], w_up[0], w_down[0],
     )
 
 

time: 143 us -> 136 us (0.951)
  local copies, waits for them, and re-layouts: 6.85 us -> 1.88 us
    unnamed x7 -> x1, local copies, waits for them, and re-layouts: 3.41 us -> 1.88 us
    broadcast_in_dim x1 -> x0, local copies, waits for them, and re-layouts: 1.52 us -> none  [shards(): jnp.broadcast_to(segments[:, None], (tok_dev, lanes))]
where the time goes in v3:
time: 136 us
  Pallas kernels  134 us (99%)
  local copies, waits for them, and re-layouts  1.88 us (1%)
    pallas_call x1, Pallas kernels, shards(): pl.pallas_call(functools.partial(layer_kernel, experts_n, columns, capaci...  134 us

profile of v3, /device:TPU:0, one launch (start us, length us, event | category | flops | bytes accessed | tf_op | source)
XLA Modules:
  0.0 136.0 jit_solution(12966938608821017847)
XLA Ops:
  0.0 134.1 %shard_map.136 = bf16[128,2048]{1,0:T(8,128)(2,1)} custom-call(bf16[128,2048]{1,0:T(8,128)(2,1)} %residual_ref.1, bf16[512,256]{1,0:T(8,128)(2,1)} %value_ref.1, bf16[512,256]{1,0:T(8,128)(2,1)} %gate_ref.1, s32[4,128]{1,0:T(4,128)} %bitcast.15, f32[31,256]{1,0:T(8,128)} %conv_w_ref.1, f32[1,256]{1,0:T(1,128)} %bitcast.16, f32[1,256]{1,0:T(1,128)} %bitcast.17, ...), custom_call_target="tpu_custom_call" | custom-call | tf_op jit(solution)/shard_map/pallas_call | solution.py:415
  134.1 1.9 %copy.16 = bf16[128,2048]{1,0:T(8,128)(2,1)} copy(bf16[128,2048]{1,0:T(8,128)(2,1)} %shard_map.136) | data formatting | bytes 1048576
